TPU v7x, 32 devices: a whole 2x2x4 slice. The times are simulated.
32 devices in a mesh: sp: 32 (over z, y, x, core), tp: 1.
Axes of the slice: x: 2, y: 2, z: 4, core: 2. Of those that a mesh axis runs over, the one named last changes fastest.
Arguments:
- queries: bfloat16 [8192, 1024], P('sp', 'tp'), may hold values from -30 to 30
- keys: bfloat16 [8192, 256], P('sp', 'tp'), may hold values from -30 to 30
- values: bfloat16 [8192, 256], P('sp', 'tp'), may hold values from -20 to 20
- gate_totals: float32 [8192, 16], P('sp', 'tp'), may hold values from -8192 to 0, as said below
- documents: int32 [8192], P('sp'), may hold values from 0 to 1, never falling along the last dimension, each value on 1 to 6144 neighbouring positions
- stream: bfloat16 [8192, 2048], P(('sp', 'tp')), may hold values from -3 to 3
- out_weight: bfloat16 [1024, 2048], replicated, may hold values from -0.1875 to 0.1875
- norm_gain: float32 [2048], replicated, may hold values from 0.1 to 1.9
- routes: int32 [8192, 2], P(('sp', 'tp')), may hold values from 0 to 31, all different within a row; in each aligned block of 256 rows (0 to 255, 256 to 511, ...) at most 32 rows name the same one
- route_weights: float32 [8192, 2], P(('sp', 'tp')), may hold values from 0.2 to 1
- expert_gate: bfloat16 [32, 2048, 1024], P('sp', None, 'tp'), may hold values from -0.125 to 0.125
- expert_up: bfloat16 [32, 2048, 1024], P('sp', None, 'tp'), may hold values from -0.125 to 0.125
- expert_down: bfloat16 [32, 1024, 2048], P('sp', 'tp'), may hold values from -0.1875 to 0.1875
Outputs:
- output: bfloat16 [8192, 2048], P(('sp', 'tp'))
Inputs may be any that keep to these rules, and one draw needn't show every extreme that they name: `gate_totals`: along positions it never rises, for every head. `routes`: in each aligned block of rows held by one device, no expert is named by more than 32 rows.
All inputs are finite; a program needn't handle non-finite values.
Results may differ from a plain program's by a relative error of at most 0.014.
Values may be sent and summed in bfloat16 or wider, within the bound.
A program may use at most 128 MiB of HBM per device.

v0:
```python
import functools
import math

import jax
import jax.numpy as jnp
from jax import lax
from jax.experimental import pallas as pl
from jax.experimental.pallas import tpu as pltpu
from jax.sharding import PartitionSpec as P

QUERY_HEAD_COUNT = 16
KV_HEADS = 4
HD = 64
TOP = 2


EPS = 1e-06
MASKED = -1e30


def make_fold(query_rows, query_gate, key_gate_all, query_docs, first_pos, kv_local, group):
    count = query_rows.shape[0]
    scale = HD ** (-0.5)
    query_blk = query_rows.reshape(count, kv_local, group, HD)
    gate_here = query_gate.T.reshape(kv_local, group, count, 1)
    query_pos = first_pos + jnp.arange(count, dtype=jnp.int32)
    last_pos = first_pos + count - 1
    first_doc = query_docs[0]

    def block_step(carry, block_in):
        running_max, running_sum, carried = carry
        key_block, value_block, doc_block, pos_block = block_in
        width = key_block.shape[0]

        def compute(unused):
            key_heads = key_block.reshape(width, kv_local, HD)
            value_heads = value_block.reshape(width, kv_local, HD)
            gate_keys = lax.dynamic_slice_in_dim(key_gate_all, pos_block[0], width, 0).T.reshape(
                kv_local, group, 1, width
            )
            scores = (
                jnp.einsum(
                    "qkgd,nkd->kgqn", query_blk, key_heads, preferred_element_type=jnp.float32
                )
                * scale
                + gate_here
                - gate_keys
            )
            allowed = (pos_block[None, :] <= query_pos[:, None]) & (
                doc_block[None, :] == query_docs[:, None]
            )
            scores = jnp.where(allowed, scores, MASKED)
            new_max = jnp.maximum(running_max, jnp.max(scores, axis=-1))
            weights = jnp.where(allowed, jnp.exp(scores - new_max[..., None]), 0.0)
            factor = jnp.exp(running_max - new_max)
            new_sum = running_sum * factor + jnp.sum(weights, axis=-1)
            new_carried = carried * factor[..., None] + jnp.einsum(
                "kgqn,nkd->kgqd",
                weights.astype(jnp.bfloat16),
                value_heads,
                preferred_element_type=jnp.float32,
            )
            return (new_max, new_sum, new_carried)

        skipped = (pos_block[0] > last_pos) | (doc_block[width - 1] < first_doc)
        return (lax.cond(skipped, lambda unused: carry, compute, 0), None)

    def fold(carry, piece, start):
        key_piece, value_piece, doc_piece = piece
        length = key_piece.shape[0]
        width = math.gcd(length, 512)
        blocks_count = length // width
        pos_piece = jnp.arange(length, dtype=jnp.int32)
        blocks = (
            key_piece.reshape(blocks_count, width, -1),
            value_piece.reshape(blocks_count, width, -1),
            doc_piece.reshape(blocks_count, width),
            pos_piece.reshape(blocks_count, width),
        )
        carry, unused = lax.scan(block_step, carry, blocks)
        return carry

    initial = (
        jnp.full((kv_local, group, count), MASKED, jnp.float32),
        jnp.zeros((kv_local, group, count), jnp.float32),
        jnp.zeros((kv_local, group, count, HD), jnp.float32),
    )
    return (fold, initial)


def finish(running_sum, carried):
    mixed = carried / running_sum[..., None]
    count = mixed.shape[2]
    return jnp.transpose(mixed, (2, 0, 1, 3)).reshape(count, -1).astype(jnp.bfloat16)


def shards(
    queries,
    keys,
    values,
    gate_totals,
    documents,
    stream,
    out_weight,
    norm_gain,
    routes,
    route_weights,
    expert_gate,
    expert_up,
    expert_down,
):
    tp_count = lax.axis_size("tp")
    sp_count = lax.axis_size("sp")
    tp_index = lax.axis_index("tp")
    sp_index = lax.axis_index("sp")
    group = QUERY_HEAD_COUNT // KV_HEADS
    tok_local = queries.shape[0]
    own_rows = tok_local // tp_count
    first_row = sp_index * tok_local
    query_rows = lax.all_to_all(queries, "tp", split_axis=0, concat_axis=1, tiled=True)
    key_whole, value_whole = (
        lax.all_gather(keys, "tp", axis=1, tiled=True),
        lax.all_gather(values, "tp", axis=1, tiled=True),
    )
    gate_whole = lax.all_gather(gate_totals, "tp", axis=1, tiled=True)
    key_gate_all = lax.all_gather(gate_whole, "sp", axis=0, tiled=True)
    query_gate = lax.dynamic_slice_in_dim(gate_whole, tp_index * own_rows, own_rows, 0)
    query_docs = lax.dynamic_slice_in_dim(documents, tp_index * own_rows, own_rows, 0)
    fold, initial = make_fold(
        query_rows,
        query_gate,
        key_gate_all,
        query_docs,
        first_row + tp_index * own_rows,
        KV_HEADS,
        group,
    )
    running_max, running_sum, carried = fold(
        initial,
        (
            lax.all_gather(key_whole, "sp", axis=0, tiled=True),
            lax.all_gather(value_whole, "sp", axis=0, tiled=True),
            lax.all_gather(documents, "sp", axis=0, tiled=True),
        ),
        jnp.int32(0),
    )
    attended = finish(running_sum, carried)
    hidden = (
        stream.astype(jnp.float32)
        + jnp.dot(attended, out_weight, preferred_element_type=jnp.float32)
    ).astype(jnp.bfloat16)
    hidden_f = hidden.astype(jnp.float32)
    normed = (
        hidden_f
        * lax.rsqrt(jnp.mean(hidden_f * hidden_f, axis=-1, keepdims=True) + EPS)
        * norm_gain
    ).astype(jnp.bfloat16)
    local_experts = expert_gate.shape[0]
    experts_total = local_experts * sp_count
    capacity = max(2, 2 * tok_local * TOP // (tp_count * experts_total))
    flat = routes.reshape(-1)
    hits = (flat[:, None] == jnp.arange(experts_total, dtype=jnp.int32)[None, :]).astype(jnp.int32)
    slot_index = jnp.sum(jnp.cumsum(hits, axis=0) * hits, axis=1) - 1
    target = flat * capacity + slot_index
    entry_rows = jnp.repeat(normed, TOP, axis=0)
    outgoing = (
        jnp.zeros((experts_total * capacity, normed.shape[1]), jnp.bfloat16)
        .at[target]
        .set(entry_rows)
    )
    outgoing = outgoing.reshape(experts_total, capacity, -1)
    arrived = lax.all_to_all(outgoing, "sp", split_axis=0, concat_axis=0, tiled=True)
    slots = arrived.shape[1]
    both_halves = lax.all_gather(arrived, "tp", axis=0, tiled=True)
    grouped = both_halves.reshape(tp_count * sp_count, local_experts, slots, -1)
    gate = jnp.einsum("secd,edf->secf", grouped, expert_gate, preferred_element_type=jnp.float32)
    upper = jnp.einsum("secd,edf->secf", grouped, expert_up, preferred_element_type=jnp.float32)
    inner = (jax.nn.silu(gate) * upper).astype(jnp.bfloat16)
    partial_value = jnp.einsum(
        "secf,efd->secd", inner, expert_down, preferred_element_type=jnp.float32
    )
    partial_value = lax.optimization_barrier(partial_value.astype(jnp.bfloat16)).astype(jnp.float32)
    summed = lax.psum_scatter(
        partial_value.reshape(tp_count * sp_count * local_experts, slots, -1).astype(jnp.bfloat16),
        "tp",
        scatter_dimension=0,
        tiled=True,
    )
    returned = lax.all_to_all(summed, "sp", split_axis=0, concat_axis=0, tiled=True)
    answers = returned.reshape(experts_total * capacity, -1)[target].reshape(own_rows, TOP, -1)
    routed = jnp.sum(route_weights[..., None] * answers.astype(jnp.float32), axis=1)
    return (hidden_f + routed).astype(jnp.bfloat16)


def attend_kernel(sub, span, width, query_ref, kv_ref, notes_ref, out_ref, boundary_ref):
    tile = pl.program_id(0)
    stripes = kv_ref.shape[0]
    stripe = lax.rem(lax.axis_index("sp"), stripes)
    blocks = query_ref.shape[0]
    block = span // blocks
    group = QUERY_HEAD_COUNT // KV_HEADS
    rows = blocks * sub

    @pl.when(tile == 0)
    def count():
        earlier = notes_ref[:, :, group:group + 1, :] < 0.5
        boundary_ref[0] = jnp.sum(earlier.astype(jnp.float32)).astype(jnp.int32)

    boundary = boundary_ref[0]
    first = tile * span
    per_tile = span // width
    taken = width // block
    zeros = jnp.zeros((rows, HD), jnp.bfloat16)
    query = query_ref[...].reshape(rows, group * HD) * jnp.bfloat16(HD ** (-0.5))
    stacked = jnp.concatenate(
        [
            jnp.concatenate([query[:, head * HD:(head + 1) * HD], zeros], axis=1)
            for head in range(group)
        ],
        axis=0,
    )
    row = lax.broadcasted_iota(jnp.int32, (rows, 1), 0)
    query_pos = first + (row // sub) * block + stripe * sub + lax.rem(row, sub)
    doc_start = jnp.where(query_pos >= boundary, boundary, 0)
    per_z = stripes // taken

    def gate_rows(index):
        block_notes = notes_ref[pl.ds(lax.rem(index, per_z) * taken, taken), index // per_z]
        return [
            jnp.concatenate(
                [block_notes[at, head:head + 1, :] for at in range(taken)], axis=1
            )
            for head in range(group)
        ]

    origin = [gate[:, 0:1] for gate in gate_rows(tile * per_tile)]
    lane = lax.broadcasted_iota(jnp.int32, (width, 2 * HD), 1)

    def chunk(index, carry, masked):
        kv = kv_ref[pl.ds(lax.rem(index, per_z) * taken, taken), index // per_z]
        kv = kv.reshape(width, 2 * HD)
        bias = [start - gate for start, gate in zip(origin, gate_rows(index))]
        if masked:
            key_pos = index * width + lax.broadcasted_iota(jnp.int32, (1, width), 1)
            allowed = (key_pos <= query_pos) & (key_pos >= doc_start)
        scores = lax.dot_general(
            stacked, kv, (((1,), (1,)), ((), ())), preferred_element_type=jnp.float32
        )
        tops, mixed = carry
        new_tops, factors, weights = [], [], []
        for head in range(group):
            score = scores[head * rows:(head + 1) * rows] + bias[head]
            if masked:
                score = jnp.where(allowed, score, MASKED)
            new_top = jnp.maximum(tops[head], jnp.max(score, axis=1, keepdims=True))
            weight = jnp.exp(score - new_top)
            factor = jnp.exp(tops[head] - new_top)
            new_tops.append(new_top)
            factors.append(factor)
            weights.append(weight.astype(jnp.bfloat16))
        mixed = mixed * jnp.concatenate(factors, axis=0) + jnp.dot(
            jnp.concatenate(weights, axis=0),
            jnp.where(lane < HD, jnp.bfloat16(1), kv),
            preferred_element_type=jnp.float32,
        )
        return (tuple(new_tops), mixed)

    carry = (
        tuple(jnp.full((rows, 1), 0.5 * MASKED, jnp.float32) for unused in range(group)),
        jnp.zeros((group * rows, 2 * HD), jnp.float32),
    )
    own = tile * per_tile
    inside = (boundary > first) & (boundary < first + span)
    second = first >= boundary
    low = jnp.where(second, boundary // width, 0)
    clean_low = jnp.where(inside, own, jnp.where(second, (boundary + width - 1) // width, 0))
    clean_low = jnp.minimum(clean_low, own)
    carry = lax.fori_loop(low, clean_low, lambda i, c: chunk(i, c, True), carry)
    carry = lax.fori_loop(clean_low, own, lambda i, c: chunk(i, c, False), carry)
    carry = lax.fori_loop(own, own + per_tile, lambda i, c: chunk(i, c, True), carry)
    unused, mixed = carry
    ratio = mixed[:, HD:] / mixed[:, :HD]
    parts = [ratio[head * rows:(head + 1) * rows] for head in range(group)]
    out_ref[...] = jnp.concatenate(parts, axis=1).astype(jnp.bfloat16).reshape(out_ref.shape)


def exchange_kernel(
    stripes,
    keys_ref,
    values_ref,
    query_ref,
    notes_ref,
    kv_all_ref,
    got_ref,
    notes_all_ref,
    kv_ref,
    z_send,
    z_recv,
    p_send,
    p_recv,
    s_send,
    s_recv,
    q_send,
    q_recv,
):
    total, sub, wide = got_ref.shape
    planes = total // stripes
    chips = stripes // 2
    me = lax.axis_index("sp")
    plane, spot = me // stripes, lax.rem(me, stripes)
    chip, core = spot // 2, lax.rem(spot, 2)
    partner = plane * stripes + chip * 2 + (1 - core)
    barrier = pltpu.get_barrier_semaphore()

    def greet(r, carry):
        pl.semaphore_signal(barrier, inc=1, device_id={"sp": lax.rem(me + r, total)})
        return carry

    lax.fori_loop(1, total, greet, 0)
    for g in range(planes):
        part = slice(g * HD, (g + 1) * HD)
        kv_ref[g] = jnp.concatenate([keys_ref[:, part], values_ref[:, part]], axis=1)
    pl.semaphore_wait(barrier, total - 1)
    sources, targets = (kv_ref, notes_ref), (kv_all_ref, notes_all_ref)

    def along(r, n):
        other = lax.rem(plane + r, planes)
        return pltpu.make_async_remote_copy(
            src_ref=sources[n].at[other],
            dst_ref=targets[n].at[spot, plane],
            send_sem=z_send.at[n, r],
            recv_sem=z_recv.at[n, r],
            device_id={"sp": other * stripes + spot},
        )

    def origin(r):
        return lax.rem(plane + planes - r, planes)

    def block(r, n):
        if r == 0:
            return sources[n].at[plane]
        return targets[n].at[spot, origin(r)]

    def across(r, m, n):
        target = lax.rem(chip + m, chips)
        return pltpu.make_async_remote_copy(
            src_ref=block(r, n),
            dst_ref=targets[n].at[spot, origin(r)],
            send_sem=p_send.at[n, r, m],
            recv_sem=p_recv.at[n, r, m],
            device_id={"sp": plane * stripes + target * 2 + core},
        )

    def over(r, m, n):
        source = lax.rem(chip + chips - m, chips) * 2 + core
        where = targets[n].at[source, origin(r)]
        return pltpu.make_async_remote_copy(
            src_ref=block(r, n) if m == 0 else where,
            dst_ref=where,
            send_sem=s_send.at[n, r, m],
            recv_sem=s_recv.at[n, r, m],
            device_id={"sp": partner},
        )

    def piece(other):
        head, stripe = other // stripes, lax.rem(other, stripes)
        return (
            pl.ds(pl.multiple_of(stripe * sub, sub), sub),
            pl.ds(pl.multiple_of(head * wide, wide), wide),
        )

    def direct(r):
        other = lax.rem(me + r, total)
        return pltpu.make_async_remote_copy(
            src_ref=query_ref.at[piece(other)],
            dst_ref=got_ref.at[me],
            send_sem=q_send.at[r],
            recv_sem=q_recv.at[r],
            device_id={"sp": other},
        )

    both = (0, 1)
    order = sorted(range(1, planes), key=lambda r: min(r, planes - r))
    for r in order:
        for n in both:
            along(r, n).start()
    for m in range(1, chips):
        for n in both:
            across(0, m, n).start()
    for n in both:
        over(0, 0, n).start()

    def send_query(r, carry):
        direct(r).start()
        return carry

    lax.fori_loop(1, total, send_query, 0)
    kv_all_ref[spot, plane] = kv_ref[plane]
    notes_all_ref[spot, plane] = notes_ref[plane]
    got_ref[me] = query_ref[piece(me)]
    for at, r in enumerate(order):
        for n in both:
            along(r, n).wait_recv()
            for m in range(1, chips):
                across(r, m, n).start()
            over(r, 0, n).start()
        earlier = 0 if at == 0 else order[at - 1]
        for m in range(1, chips):
            for n in both:
                across(earlier, m, n).wait_recv()
                over(earlier, m, n).start()
    for m in range(1, chips):
        for n in both:
            across(order[-1], m, n).wait_recv()
            over(order[-1], m, n).start()
    for n in both:
        for r in range(planes):
            for m in range(chips):
                over(r, m, n).wait()
        for r in range(1, planes):
            along(r, n).wait_send()
        for r in range(planes):
            for m in range(1, chips):
                across(r, m, n).wait_send()

    def end_query(r, carry):
        direct(r).wait()
        return carry

    lax.fori_loop(1, total, end_query, 0)


def exchange(keys, values, queries, notes, stripes):
    planes, chips = notes.shape[0], stripes // 2
    total, tok = planes * stripes, keys.shape[0]
    got = (total, tok // stripes, queries.shape[1] // planes)
    vmem = pl.BlockSpec(memory_space=pltpu.VMEM)
    dma = pltpu.SemaphoreType.DMA
    return pl.pallas_call(
        functools.partial(exchange_kernel, stripes),
        in_specs=[vmem] * 4,
        out_specs=[vmem] * 3,
        out_shape=[
            jax.ShapeDtypeStruct((stripes, planes, tok, 2 * HD), keys.dtype),
            jax.ShapeDtypeStruct(got, queries.dtype),
            jax.ShapeDtypeStruct((stripes,) + notes.shape, notes.dtype),
        ],
        scratch_shapes=[
            pltpu.VMEM((planes, tok, 2 * HD), keys.dtype),
            dma((2, planes)),
            dma((2, planes)),
            dma((2, planes, chips)),
            dma((2, planes, chips)),
            dma((2, planes, chips)),
            dma((2, planes, chips)),
            dma((total,)),
            dma((total,)),
        ],
        compiler_params=pltpu.CompilerParams(
            collective_id=0, has_side_effects=True, vmem_limit_bytes=24 * 1024 * 1024
        ),
        name="exchange",
    )(keys, values, queries, notes)


def mixture_kernel(
    capacity,
    stripes,
    slots,
    mixed_ref,
    stream_ref,
    gain_ref,
    rows_ref,
    columns_ref,
    weights_ref,
    begin_row_ref,
    begin_ref,
    project_hbm,
    gate_hbm,
    up_hbm,
    down_hbm,
    out_ref,
    project_w,
    gate_w,
    up_w,
    down_w,
    attended,
    hidden_ref,
    normed_ref,
    packed,
    landed,
    sending,
    arrived,
    inner,
    answers,
    returned,
    got,
    total,
    w_sem,
    h_send,
    h_recv,
    z_send,
    z_recv,
    a_send,
    a_recv,
    b_send,
    b_recv,
    r_send,
    r_recv,
):
    planes = begin_ref.shape[0]
    devices = planes * stripes
    tok, width = stream_ref.shape
    sub, wide = mixed_ref.shape[1:]
    backing = landed
    hidden_units = gate_w.shape[1]
    rows = stripes * slots
    step = math.gcd(width, 256)
    me = lax.axis_index("sp")
    plane, spot = me // stripes, lax.rem(me, stripes)

    def plane_of(m):
        if m == 1:
            return plane + 1 - 2 * lax.rem(plane, 2)
        if m == 2:
            return lax.rem(plane + 2, 4)
        return plane if m == 0 else 3 - plane

    barrier = pltpu.get_barrier_semaphore()

    def greet(r, carry):
        pl.semaphore_signal(barrier, inc=1, device_id={"sp": lax.rem(me + r, devices)})
        return carry

    lax.fori_loop(1, devices, greet, 0)
    weights = [
        pltpu.make_async_copy(source, target, w_sem.at[at])
        for at, (source, target) in enumerate(
            (
                (project_hbm, project_w),
                (gate_hbm.at[0], gate_w),
                (up_hbm.at[0], up_w),
                (down_hbm.at[0], down_w),
            )
        )
    ]
    for copy in weights:
        copy.start()
    pl.semaphore_wait(barrier, devices - 1)

    def home(owner):
        head, stripe = owner // stripes, lax.rem(owner, stripes)
        return (
            pl.ds(pl.multiple_of(stripe * sub, sub), sub),
            pl.ds(pl.multiple_of(head * wide, wide), wide),
        )

    def home_copy(r):
        other = lax.rem(me + r, devices)
        return pltpu.make_async_remote_copy(
            src_ref=mixed_ref.at[other],
            dst_ref=attended.at[home(me)],
            send_sem=h_send.at[r],
            recv_sem=h_recv.at[r],
            device_id={"sp": other},
        )

    def send_home(r, carry):
        home_copy(r).start()
        return carry

    def wait_home(r, carry):
        home_copy(r).wait()
        return carry

    lax.fori_loop(1, devices, send_home, 0)
    attended[home(me)] = mixed_ref[me]
    lax.fori_loop(1, devices, wait_home, 0)
    weights[0].wait()

    def project(index, squares):
        cols = pl.ds(pl.multiple_of(index * step, step), step)
        product = jnp.dot(attended[...], project_w[:, cols], preferred_element_type=jnp.float32)
        hidden = (stream_ref[:, cols].astype(jnp.float32) + product).astype(jnp.bfloat16)
        hidden_ref[:, cols] = hidden
        wider = hidden.astype(jnp.float32)
        return squares + jnp.sum(wider * wider, axis=1, keepdims=True)

    squares = lax.fori_loop(0, width // step, project, jnp.zeros((tok, 1), jnp.float32))
    inverse = lax.rsqrt(squares / width + EPS)

    def columns(body, length, size):
        def at(index, carry):
            body(pl.ds(pl.multiple_of(index * size, size), size))
            return carry

        lax.fori_loop(0, length // size, at, 0)

    def dot(left, right):
        return jnp.dot(left, right, preferred_element_type=jnp.float32)

    def norm(cols):
        scaled = hidden_ref[:, cols].astype(jnp.float32) * inverse * gain_ref[:, cols]
        normed_ref[:, cols] = scaled.astype(jnp.bfloat16)

    columns(norm, width, step)
    high_slot = lax.broadcasted_iota(jnp.int32, (capacity, 1), 0)
    low_slot = lax.broadcasted_iota(jnp.int32, (1, capacity), 1)

    def chosen_of(hit):
        return jnp.where(hit, 1.0, 0.0)

    def out_copy(m):
        return pltpu.make_async_remote_copy(
            src_ref=packed.at[m],
            dst_ref=landed.at[m],
            send_sem=z_send.at[m],
            recv_sem=z_recv.at[m],
            device_id={"sp": plane_of(m) * stripes + spot},
        )

    def back_copy(m):
        return pltpu.make_async_remote_copy(
            src_ref=backing.at[m],
            dst_ref=got.at[m],
            send_sem=r_send.at[m],
            recv_sem=r_recv.at[m],
            device_id={"sp": plane_of(m) * stripes + spot},
        )

    def near_copy(source, target, send, recv, m, i):
        other = lax.rem(spot + i, stripes)
        return pltpu.make_async_remote_copy(
            src_ref=source.at[m, other],
            dst_ref=target.at[m, spot],
            send_sem=send.at[m, i],
            recv_sem=recv.at[m, i],
            device_id={"sp": plane * stripes + other},
        )

    def to_expert(m, i):
        return near_copy(sending, arrived, a_send, a_recv, m, i)

    def from_expert(m, i):
        return near_copy(answers, returned, b_send, b_recv, m, i)

    def pack(m):
        begins = plane_of(m) * rows
        hits = sum(chosen_of(rows_ref[k:k + 1] - begins == high_slot) for k in range(TOP))
        hits = hits.astype(jnp.bfloat16)

        def body(cols):
            packed[m, :, cols] = dot(hits, normed_ref[:, cols]).astype(jnp.bfloat16)

        columns(body, width, step)

    def spread(m):
        hits = chosen_of(begin_ref[plane_of(m)] == low_slot).astype(jnp.bfloat16)
        source = packed if m == 0 else landed
        if m:
            out_copy(m).wait_recv()

        def body(cols):
            chosen = dot(hits, source[m, :, cols]).astype(jnp.bfloat16)
            sending[m, :, :, cols] = chosen.reshape(stripes, slots, step)

        columns(body, width, step)
        arrived[m, spot] = sending[m, spot]
        for i in range(1, stripes):
            to_expert(m, i).start()

    def compute(m):
        for i in range(1, stripes):
            to_expert(m, i).wait_recv()

        def middle(cols):
            rows_in = arrived[m].reshape(rows, width)
            gate = dot(rows_in, gate_w[:, cols])
            upper = dot(rows_in, up_w[:, cols])
            inner[:, cols] = (jax.nn.silu(gate) * upper).astype(jnp.bfloat16)

        columns(middle, hidden_units, math.gcd(hidden_units, 256))

        def last(cols):
            answer = dot(inner[...], down_w[:, cols]).astype(jnp.bfloat16)
            answers[m, :, :, cols] = answer.reshape(stripes, slots, step)

        columns(last, width, step)
        returned[m, spot] = answers[m, spot]
        for i in range(1, stripes):
            from_expert(m, i).start()

    def collect(m):
        hits = chosen_of(begin_row_ref[plane_of(m)] == high_slot).astype(jnp.bfloat16)
        for i in range(1, stripes):
            from_expert(m, i).wait_recv()
        target = got if m == 0 else backing

        def body(cols):
            source = returned[m, :, :, cols].reshape(rows, step)
            target[m, :, cols] = dot(hits, source).astype(jnp.bfloat16)

        columns(body, width, step)
        if m:
            back_copy(m).start()

    def combine(m, first, final):
        begins = plane_of(m) * rows
        share = sum(
            jnp.where(columns_ref[:, k:k + 1] - begins == low_slot, weights_ref[:, k:k + 1], 0.0)
            for k in range(TOP)
        )
        high = share.astype(jnp.bfloat16)
        low = (share - high.astype(jnp.float32)).astype(jnp.bfloat16)
        if m:
            back_copy(m).wait_recv()

        def body(cols):
            rows_got = got[m, :, cols]
            term = dot(high, rows_got) + dot(low, rows_got)
            base = hidden_ref[:, cols].astype(jnp.float32) if first else total[:, cols]
            if final:
                out_ref[:, cols] = (base + term).astype(jnp.bfloat16)
            else:
                total[:, cols] = base + term

        columns(body, width, step)

    pack(2)
    pack(1)
    out_copy(2).start()
    pack(3)
    out_copy(1).start()
    pack(0)
    out_copy(3).start()
    spread(0)
    for copy in weights[1:]:
        copy.wait()
    compute(0)
    spread(2)
    collect(0)
    combine(0, True, False)
    compute(2)
    spread(1)
    collect(2)
    compute(1)
    spread(3)
    collect(1)
    compute(3)
    collect(3)
    combine(1, False, False)
    combine(2, False, False)
    combine(3, False, True)
    for m in range(planes):
        if m:
            out_copy(m).wait_send()
            back_copy(m).wait_send()
        for i in range(1, stripes):
            to_expert(m, i).wait_send()
            from_expert(m, i).wait_send()


def mixture(capacity, stripes, slots, operands):
    mixed, stream, begin, out_weight, expert_gate, expert_up, expert_down = (
        operands[0],
        operands[1],
        operands[7],
        *operands[8:],
    )
    tok, width = stream.shape
    planes = begin.shape[0]
    vmem = pl.BlockSpec(memory_space=pltpu.VMEM)
    anywhere = pl.BlockSpec(memory_space=pl.ANY)
    dma = pltpu.SemaphoreType.DMA
    block = pltpu.VMEM((planes, capacity, width), jnp.bfloat16)
    wide = pltpu.VMEM((planes, stripes, slots, width), jnp.bfloat16)
    return pl.pallas_call(
        functools.partial(mixture_kernel, capacity, stripes, slots),
        in_specs=[vmem] * 8 + [anywhere] * 4,
        out_specs=vmem,
        out_shape=jax.ShapeDtypeStruct((tok, width), jnp.bfloat16),
        scratch_shapes=[
            pltpu.VMEM(out_weight.shape, jnp.bfloat16),
            pltpu.VMEM(expert_gate.shape[1:], jnp.bfloat16),
            pltpu.VMEM(expert_up.shape[1:], jnp.bfloat16),
            pltpu.VMEM(expert_down.shape[1:], jnp.bfloat16),
            pltpu.VMEM((tok, out_weight.shape[0]), jnp.bfloat16),
            pltpu.VMEM((tok, width), jnp.bfloat16),
            pltpu.VMEM((tok, width), jnp.bfloat16),
            block,
            block,
            wide,
            wide,
            pltpu.VMEM((stripes * slots, expert_gate.shape[2]), jnp.bfloat16),
            wide,
            wide,
            block,
            pltpu.VMEM((tok, width), jnp.float32),
            dma((4,)),
            dma((planes * stripes,)),
            dma((planes * stripes,)),
            dma((planes,)),
            dma((planes,)),
            dma((planes, stripes)),
            dma((planes, stripes)),
            dma((planes, stripes)),
            dma((planes, stripes)),
            dma((planes,)),
            dma((planes,)),
        ],
        compiler_params=pltpu.CompilerParams(
            collective_id=1 + capacity // 16,
            has_side_effects=True,
            vmem_limit_bytes=63 * 1024 * 1024,
        ),
        name="mixture",
    )(*operands)


def fast_shards(
    queries,
    keys,
    values,
    gate_totals,
    documents,
    stream,
    out_weight,
    norm_gain,
    routes,
    route_weights,
    expert_gate,
    expert_up,
    expert_down,
):
    sp_count = lax.axis_size("sp")
    group = QUERY_HEAD_COUNT // KV_HEADS
    tok = queries.shape[0]
    stripes = sp_count // KV_HEADS
    sub = tok // stripes
    blocks = 4
    span = blocks * tok
    width = min(span, 1024)
    tiles = sp_count // blocks
    slots = max(2, 2 * tok * TOP // sp_count)
    flat = jnp.transpose(routes).reshape(-1)
    hits = (flat[:, None] == jnp.arange(sp_count, dtype=jnp.int32)[None, :]).astype(jnp.int32)
    slot_index = jnp.sum(jnp.cumsum(hits, axis=0) * hits, axis=1) - 1
    own_counts = jnp.sum(hits, axis=0).reshape(KV_HEADS, stripes)
    own_offsets = jnp.cumsum(own_counts, axis=1) - own_counts
    position = (slot_index + jnp.sum(hits * own_offsets.reshape(1, -1), axis=1)).reshape(TOP, tok)
    owner = (flat // stripes).reshape(TOP, tok)
    full = stripes * slots
    place = owner * full + position
    largest = jnp.max(jnp.sum(own_counts, axis=1))
    pad = jnp.zeros((KV_HEADS, 1, tok - stripes), jnp.int32)
    told = [
        jnp.broadcast_to(documents[None, None, :], (KV_HEADS, 1, tok)),
        jnp.concatenate([own_counts[:, None, :], pad], axis=2),
        jnp.broadcast_to(largest, (KV_HEADS, 1, tok)),
        jnp.zeros((KV_HEADS, 1, tok), jnp.int32),
    ]
    notes = jnp.concatenate(
        [jnp.transpose(gate_totals).reshape(KV_HEADS, group, tok)]
        + [line.astype(jnp.float32) for line in told],
        axis=1,
    )
    kv_all, query_got, notes_all = exchange(keys, values, queries, notes, stripes)
    worst = jnp.max(notes_all[:, :, group + 2, 0]).astype(jnp.int32)
    spot = lax.rem(lax.axis_index("sp"), stripes)
    counts = lax.dynamic_index_in_dim(notes_all, spot, 0, keepdims=False)
    counts = counts[:, group + 1, :stripes].astype(jnp.int32)
    offsets = jnp.cumsum(counts, axis=1) - counts
    number = jnp.arange(slots, dtype=jnp.int32)[None, None, :]
    begin = jnp.where(number < counts[:, :, None], offsets[:, :, None] + number, -1)
    begin = begin.reshape(KV_HEADS, full)
    mixed = pl.pallas_call(
        functools.partial(attend_kernel, sub, span, width),
        grid=(tiles,),
        in_specs=[
            pl.BlockSpec((blocks, sub, group * HD), lambda i: (i, 0, 0)),
            pl.BlockSpec(kv_all.shape, lambda i: (0, 0, 0, 0)),
            pl.BlockSpec(notes_all.shape, lambda i: (0, 0, 0, 0)),
        ],
        out_specs=pl.BlockSpec((blocks, sub, group * HD), lambda i: (i, 0, 0)),
        out_shape=jax.ShapeDtypeStruct((sp_count, sub, group * HD), jnp.bfloat16),
        scratch_shapes=[pltpu.SMEM((1,), jnp.int32)],
        compiler_params=pltpu.CompilerParams(vmem_limit_bytes=48 * 1024 * 1024),
        name="attend",
    )(query_got, kv_all, notes_all)
    sizes = (full * 5 // 8, full * 11 // 16, full * 13 // 16, full)
    operands = (
        mixed,
        stream,
        norm_gain[None, :],
        place,
        jnp.transpose(place),
        route_weights,
        begin[:, None, :],
        begin[:, :, None],
        out_weight,
        expert_gate,
        expert_up,
        expert_down,
    )

    def sized(capacity):
        return lambda given: mixture(capacity, stripes, slots, given)

    choice = sum((worst > size).astype(jnp.int32) for size in sizes[:-1])
    return lax.switch(choice, [sized(size) for size in sizes], operands)


def solution(mesh):
    sp_count, tp_count = mesh.shape["sp"], mesh.shape["tp"]
    fast = tp_count == 1 and sp_count % (4 * KV_HEADS) == 0 and KV_HEADS == 4

    def body(*arrays):
        tok, stripes = arrays[0].shape[0], sp_count // KV_HEADS
        small = stripes * (2 * tok * TOP // sp_count) <= 256
        return (fast_shards if fast and small else shards)(*arrays)

    return jax.shard_map(
        body,
        mesh=mesh,
        in_specs=(
            P("sp", "tp"),
            P("sp", "tp"),
            P("sp", "tp"),
            P("sp", "tp"),
            P("sp"),
            P(("sp", "tp"), None),
            P(),
            P(),
            P(("sp", "tp"), None),
            P(("sp", "tp"), None),
            P("sp", None, "tp"),
            P("sp", None, "tp"),
            P("sp", "tp", None),
        ),
        out_specs=P(("sp", "tp"), None),
        check_vma=False,
    )
```

profile of v0, /device:TPU:19, one launch (start us, length us, event | category | flops | bytes accessed | tf_op | source)
XLA Modules:
  0.0 260.6 jit_solution(1814528116548650574)
XLA Ops:
  0.0 0.8 reshape.208
  0.8 0.7 convert_element_type.53
  1.5 0.7 copy.100
  2.1 0.1 convert_reduce_fusion
  2.3 0.1 broadcast_in_dim_reshape.2
  2.4 0.1 reshape.209
  2.4 0.1 reduce_sum.37
  2.6 0.6 reduce_max.18
  3.9 1.0 copy-done
  5.0 0.9 copy-done.1
  5.9 0.9 copy-done.2
  6.8 27.1 %exchange.1 = (bf16[8,4,256,128]{3,2,1,0:T(8,128)(2,1)S(1)}, bf16[32,32,256]{2,1,0:T(8,128)(2,1)S(1)}, f32[8,4,8,256]{3,2,1,0:T(8,128)S(1)}) custom-call(bf16[256,256]{1,0:T(8,128)(2,1)S(1)} %copy-done.1, bf16[256,256]{1,0:T(8,128)(2,1)S(1)} %copy-done.2, bf16[256,1024]{1,0:T(8,128)(2,1)S(1)} %copy-done, f32[4,8,256]{2,1,0:T(8,128)S(1)} %concatenate.7.notes_ref), custom_call_target="tpu_custom_call" | custom-call | tf_op jit(solution)/shard_map/exchange/pallas_call | solution.py:439
  33.9 0.6 slice_reduce_fusion.1
  35.2 30.7 %attend.1 = bf16[32,32,256]{2,1,0:T(8,128)(2,1)} custom-call(bf16[32,32,256]{2,1,0:T(8,128)(2,1)S(1)} %get-tuple-element.158.query_ref, bf16[8,4,256,128]{3,2,1,0:T(8,128)(2,1)S(1)} %get-tuple-element.159.kv_ref, f32[8,4,8,256]{3,2,1,0:T(8,128)S(1)} %get-tuple-element.157.notes_ref), custom_call_target="tpu_custom_call" | custom-call | tf_op jit(solution)/shard_map/attend/pallas_call | solution.py:876
  65.8 0.2 reduce_window_sum.36
  66.0 0.1 reduce_window_sum.37
  66.1 1.2 reduce-window.6
  67.3 0.2 slice_reduce_fusion
  67.6 0.1 fusion.1
  67.7 0.1 copy.94
  68.0 0.1 lt.66
  68.1 0.2 reduce_window_sum.38
  68.4 189.9 %conditional.1 = (bf16[256,2048]{1,0:T(8,128)(2,1)}) conditional(s32[]{:T(128)} %clamp.3, (bf16[32,32,256]{2,1,0:T(8,128)(2,1)}, bf16[256,2048]{1,0:T(8,128)(2,1)}, f32[2048]{0:T(1024)S(1)}, s32[2,256]{1,0:T(2,128)S(1)}, s32[256,2]{1,0:T(8,128)S(1)}, /*index=5*/f32[256,2]{0,1:T(2,128)S(1)}, ...), branch_computations={%region_10.11_spmd.clone, %region_11.12_spmd.clone, %region_12.13_... | conditional | flops 6144 | bytes 73872 | solution.py:910
  68.8 0.8 copy.96.weights_ref
  69.5 0.1 lt.91
  69.7 0.1 add.96
  69.8 0.6 compare_select_fusion.1.begin_row_ref
  70.4 0.5 add.110
  70.9 0.5 lt.102
  71.5 0.9 add_select_fusion.1.begin_ref
  72.3 185.3 %mixture.5 = bf16[256,2048]{1,0:T(8,128)(2,1)} custom-call(bf16[32,32,256]{2,1,0:T(8,128)(2,1)} %get-tuple-element.341.mixed_ref, bf16[256,2048]{1,0:T(8,128)(2,1)} %get-tuple-element.344.stream_ref, f32[1,2048]{1,0:T(1,128)S(1)} %bitcast.34, s32[2,256]{1,0:T(2,128)S(1)} %get-tuple-element.342.rows_ref, s32[256,2]{1,0:T(8,128)S(1)} %get-tuple-element.343.columns_ref, ...), custom_call_target="tpu_custom_call" | custom-call | tf_op jit(solution)/shard_map/cond/branch_1_fun/mixture/pallas_call | solution.py:777
  258.3 2.3 copy.107
  (30 shorter events, 0.4 us)
Async XLA Ops:
  0.0 66.1 %copy-start.5 = (s32[256,2]{0,1:T(2,128)S(1)}, s32[256,2]{0,1:T(2,128)}, u32[]{:S(2)}) copy-start(s32[256,2]{0,1:T(2,128)} %param.25) | copy-start | bytes 6148
  0.0 68.4 %copy-start.3 = (f32[2048]{0:T(1024)S(1)}, f32[2048]{0:T(1024)}, u32[]{:S(2)}) copy-start(f32[2048]{0:T(1024)} %param.24) | copy-start | bytes 24580
  0.0 68.4 %copy-start.4 = (f32[256,2]{0,1:T(2,128)S(1)}, f32[256,2]{0,1:T(2,128)}, u32[]{:S(2)}) copy-start(f32[256,2]{0,1:T(2,128)} %param.26) | copy-start | bytes 6148
  3.9 1.0 copy-start
  5.0 0.9 copy-start.1
  5.9 0.9 copy-start.2
where the time goes:
time: 260 us; the launch traced here: 261 us
  Pallas kernels  243 us (93%)
  local copies, waits for them, and re-layouts  9.66 us (4%)
  other arithmetic  5.43 us (2%)
    pallas_call x1, Pallas kernels, mixture(): pl.pallas_call(functools.partial(mixture_kernel, capacity, stripes, slots...  185 us
    pallas_call x1, Pallas kernels, fast_shards(): pl.pallas_call(functools.partial(attend_kernel, sub, span, width), grid=(...  30.7 us
    pallas_call x1, Pallas kernels, exchange(): pl.pallas_call(functools.partial(exchange_kernel, stripes), in_specs=[vme...  27.1 us
    unnamed x14, local copies, waits for them, and re-layouts  5.84 us

commit v1 on v0

--- a/solution.py
+++ b/solution.py
@@ -15,6 +15,7 @@
 
 
 EPS = 1e-06
+STEP = 1024
 MASKED = -1e30
 
 
@@ -286,14 +287,17 @@
 
 def exchange_kernel(
     stripes,
-    keys_ref,
-    values_ref,
+    keys_hbm,
+    values_hbm,
     query_ref,
     notes_ref,
     kv_all_ref,
     got_ref,
     notes_all_ref,
+    keys_ref,
+    values_ref,
     kv_ref,
+    l_sem,
     z_send,
     z_recv,
     p_send,
@@ -312,11 +316,27 @@
     partner = plane * stripes + chip * 2 + (1 - core)
     barrier = pltpu.get_barrier_semaphore()
 
+    def piece(other):
+        head, stripe = other // stripes, lax.rem(other, stripes)
+        return (
+            pl.ds(pl.multiple_of(stripe * sub, sub), sub),
+            pl.ds(pl.multiple_of(head * wide, wide), wide),
+        )
+
     def greet(r, carry):
         pl.semaphore_signal(barrier, inc=1, device_id={"sp": lax.rem(me + r, total)})
         return carry
 
     lax.fori_loop(1, total, greet, 0)
+    loads = [
+        pltpu.make_async_copy(keys_hbm, keys_ref, l_sem.at[0]),
+        pltpu.make_async_copy(values_hbm, values_ref, l_sem.at[1]),
+        pltpu.make_async_copy(query_ref.at[piece(me)], got_ref.at[me], l_sem.at[2]),
+    ]
+    for load in loads:
+        load.start()
+    for load in loads[:2]:
+        load.wait()
     for g in range(planes):
         part = slice(g * HD, (g + 1) * HD)
         kv_ref[g] = jnp.concatenate([keys_ref[:, part], values_ref[:, part]], axis=1)
@@ -360,13 +380,6 @@
             send_sem=s_send.at[n, r, m],
             recv_sem=s_recv.at[n, r, m],
             device_id={"sp": partner},
-        )
-
-    def piece(other):
-        head, stripe = other // stripes, lax.rem(other, stripes)
-        return (
-            pl.ds(pl.multiple_of(stripe * sub, sub), sub),
-            pl.ds(pl.multiple_of(head * wide, wide), wide),
         )
 
     def direct(r):
@@ -397,7 +410,7 @@
     lax.fori_loop(1, total, send_query, 0)
     kv_all_ref[spot, plane] = kv_ref[plane]
     notes_all_ref[spot, plane] = notes_ref[plane]
-    got_ref[me] = query_ref[piece(me)]
+    loads[2].wait()
     for at, r in enumerate(order):
         for n in both:
             along(r, n).wait_recv()
@@ -434,11 +447,12 @@
     planes, chips = notes.shape[0], stripes // 2
     total, tok = planes * stripes, keys.shape[0]
     got = (total, tok // stripes, queries.shape[1] // planes)
+    hbm = pl.BlockSpec(memory_space=pltpu.HBM)
     vmem = pl.BlockSpec(memory_space=pltpu.VMEM)
     dma = pltpu.SemaphoreType.DMA
     return pl.pallas_call(
         functools.partial(exchange_kernel, stripes),
-        in_specs=[vmem] * 4,
+        in_specs=[hbm, hbm, hbm, vmem],
         out_specs=[vmem] * 3,
         out_shape=[
             jax.ShapeDtypeStruct((stripes, planes, tok, 2 * HD), keys.dtype),
@@ -446,7 +460,10 @@
             jax.ShapeDtypeStruct((stripes,) + notes.shape, notes.dtype),
         ],
         scratch_shapes=[
+            pltpu.VMEM(keys.shape, keys.dtype),
+            pltpu.VMEM(values.shape, values.dtype),
             pltpu.VMEM((planes, tok, 2 * HD), keys.dtype),
+            dma((3,)),
             dma((2, planes)),
             dma((2, planes)),
             dma((2, planes, chips)),
@@ -468,18 +485,20 @@
     stripes,
     slots,
     mixed_ref,
-    stream_ref,
     gain_ref,
     rows_ref,
     columns_ref,
-    weights_ref,
     begin_row_ref,
     begin_ref,
+    stream_hbm,
+    weights_hbm,
     project_hbm,
     gate_hbm,
     up_hbm,
     down_hbm,
     out_ref,
+    stream_ref,
+    weights_ref,
     project_w,
     gate_w,
     up_w,
@@ -515,16 +534,15 @@
     backing = landed
     hidden_units = gate_w.shape[1]
     rows = stripes * slots
-    step = math.gcd(width, 256)
+    step = math.gcd(width, STEP)
     me = lax.axis_index("sp")
     plane, spot = me // stripes, lax.rem(me, stripes)
 
     def plane_of(m):
-        if m == 1:
-            return plane + 1 - 2 * lax.rem(plane, 2)
-        if m == 2:
-            return lax.rem(plane + 2, 4)
-        return plane if m == 0 else 3 - plane
+        return 2 * lax.rem(plane // 2 + m // 2, 2) + lax.rem(plane + m, 2)
+
+    def turned(q):
+        return 2 * lax.rem((q + 1) // 2, 2) + q // 2
 
     barrier = pltpu.get_barrier_semaphore()
 
@@ -537,6 +555,8 @@
         pltpu.make_async_copy(source, target, w_sem.at[at])
         for at, (source, target) in enumerate(
             (
+                (stream_hbm, stream_ref),
+                (weights_hbm, weights_ref),
                 (project_hbm, project_w),
                 (gate_hbm.at[0], gate_w),
                 (up_hbm.at[0], up_w),
@@ -576,7 +596,8 @@
     lax.fori_loop(1, devices, send_home, 0)
     attended[home(me)] = mixed_ref[me]
     lax.fori_loop(1, devices, wait_home, 0)
-    weights[0].wait()
+    for copy in weights[:3]:
+        copy.wait()
 
     def project(index, squares):
         cols = pl.ds(pl.multiple_of(index * step, step), step)
@@ -584,6 +605,7 @@
         hidden = (stream_ref[:, cols].astype(jnp.float32) + product).astype(jnp.bfloat16)
         hidden_ref[:, cols] = hidden
         wider = hidden.astype(jnp.float32)
+        total[:, cols] = wider
         return squares + jnp.sum(wider * wider, axis=1, keepdims=True)
 
     squares = lax.fori_loop(0, width // step, project, jnp.zeros((tok, 1), jnp.float32))
@@ -654,25 +676,32 @@
 
         columns(body, width, step)
 
+    def peers(act):
+        def at(i, carry):
+            act(i)
+            return carry
+
+        lax.fori_loop(1, stripes, at, 0)
+
     def spread(m):
         hits = chosen_of(begin_ref[plane_of(m)] == low_slot).astype(jnp.bfloat16)
-        source = packed if m == 0 else landed
-        if m:
+
+        @pl.when(m > 0)
+        def wait():
             out_copy(m).wait_recv()
 
         def body(cols):
-            chosen = dot(hits, source[m, :, cols]).astype(jnp.bfloat16)
+            chosen = dot(hits, landed[m, :, cols]).astype(jnp.bfloat16)
             sending[m, :, :, cols] = chosen.reshape(stripes, slots, step)
 
         columns(body, width, step)
         arrived[m, spot] = sending[m, spot]
-        for i in range(1, stripes):
-            to_expert(m, i).start()
+        peers(lambda i: to_expert(m, i).start())
+
+    def take(m):
+        peers(lambda i: to_expert(m, i).wait_recv())
 
     def compute(m):
-        for i in range(1, stripes):
-            to_expert(m, i).wait_recv()
-
         def middle(cols):
             rows_in = arrived[m].reshape(rows, width)
             gate = dot(rows_in, gate_w[:, cols])
@@ -687,24 +716,23 @@
 
         columns(last, width, step)
         returned[m, spot] = answers[m, spot]
-        for i in range(1, stripes):
-            from_expert(m, i).start()
+        peers(lambda i: from_expert(m, i).start())
 
     def collect(m):
         hits = chosen_of(begin_row_ref[plane_of(m)] == high_slot).astype(jnp.bfloat16)
-        for i in range(1, stripes):
-            from_expert(m, i).wait_recv()
-        target = got if m == 0 else backing
+        peers(lambda i: from_expert(m, i).wait_recv())
 
         def body(cols):
             source = returned[m, :, :, cols].reshape(rows, step)
-            target[m, :, cols] = dot(hits, source).astype(jnp.bfloat16)
+            backing[m, :, cols] = dot(hits, source).astype(jnp.bfloat16)
 
         columns(body, width, step)
-        if m:
+
+        @pl.when(m > 0)
+        def send():
             back_copy(m).start()
 
-    def combine(m, first, final):
+    def combine(m, final):
         begins = plane_of(m) * rows
         share = sum(
             jnp.where(columns_ref[:, k:k + 1] - begins == low_slot, weights_ref[:, k:k + 1], 0.0)
@@ -712,74 +740,114 @@
         )
         high = share.astype(jnp.bfloat16)
         low = (share - high.astype(jnp.float32)).astype(jnp.bfloat16)
-        if m:
-            back_copy(m).wait_recv()
 
         def body(cols):
             rows_got = got[m, :, cols]
-            term = dot(high, rows_got) + dot(low, rows_got)
-            base = hidden_ref[:, cols].astype(jnp.float32) if first else total[:, cols]
+            term = total[:, cols] + dot(high, rows_got) + dot(low, rows_got)
             if final:
-                out_ref[:, cols] = (base + term).astype(jnp.bfloat16)
+                out_ref[:, cols] = term.astype(jnp.bfloat16)
             else:
-                total[:, cols] = base + term
+                total[:, cols] = term
 
         columns(body, width, step)
 
-    pack(2)
-    pack(1)
-    out_copy(2).start()
-    pack(3)
-    out_copy(1).start()
-    pack(0)
-    out_copy(3).start()
-    spread(0)
-    for copy in weights[1:]:
-        copy.wait()
-    compute(0)
-    spread(2)
-    collect(0)
-    combine(0, True, False)
-    compute(2)
-    spread(1)
-    collect(2)
-    compute(1)
-    spread(3)
-    collect(1)
-    compute(3)
-    collect(3)
-    combine(1, False, False)
-    combine(2, False, False)
-    combine(3, False, True)
-    for m in range(planes):
-        if m:
+    def far_first(q):
+        return 2 * lax.rem(q + 1, 2) + lax.rem((q + 1) // 2, 2)
+
+    def fill(q, carry):
+        pack(far_first(q))
+
+        @pl.when(q > 0)
+        def send():
+            out_copy(far_first(q - 1)).start()
+
+        return carry
+
+    lax.fori_loop(0, planes, fill, 0)
+    landed[0] = packed[0]
+
+    def work(q, carry):
+        @pl.when((q > 0) & (q != 3))
+        def first():
+            collect(turned(q - 1 - q // 4))
+
+        @pl.when(q < 3)
+        def second():
+            def at(extra, inner_carry):
+                spread(turned(q + extra))
+                take_now = turned(q)
+
+                @pl.when(extra == 0)
+                def third():
+                    take(take_now)
+
+                return inner_carry
+
+            lax.fori_loop(0, 1 + q // 2, at, 0)
+
+        @pl.when(q == 0)
+        def ready():
+            for copy in weights[3:]:
+                copy.wait()
+
+        @pl.when(q == 3)
+        def last():
+            take(turned(q))
+
+        @pl.when(q < planes)
+        def fourth():
+            compute(turned(q))
+
+        return carry
+
+    lax.fori_loop(0, planes + 2, work, 0)
+    got[0] = backing[0]
+
+    def gather(q, carry):
+        m = turned(q)
+
+        @pl.when(m > 0)
+        def wait():
+            back_copy(m).wait_recv()
+
+        combine(m, False)
+        return carry
+
+    lax.fori_loop(0, planes - 1, gather, 0)
+    back_copy(1).wait_recv()
+    combine(1, True)
+
+    def finish_sends(m, carry):
+        @pl.when(m > 0)
+        def far():
             out_copy(m).wait_send()
             back_copy(m).wait_send()
-        for i in range(1, stripes):
-            to_expert(m, i).wait_send()
-            from_expert(m, i).wait_send()
+
+        peers(lambda i: to_expert(m, i).wait_send())
+        peers(lambda i: from_expert(m, i).wait_send())
+        return carry
+
+    lax.fori_loop(0, planes, finish_sends, 0)
 
 
 def mixture(capacity, stripes, slots, operands):
-    mixed, stream, begin, out_weight, expert_gate, expert_up, expert_down = (
-        operands[0],
-        operands[1],
-        operands[7],
-        *operands[8:],
-    )
+    begin = operands[5]
+    stream, route_weights, out_weight, expert_gate, expert_up, expert_down = operands[6:]
     tok, width = stream.shape
     planes = begin.shape[0]
     vmem = pl.BlockSpec(memory_space=pltpu.VMEM)
-    anywhere = pl.BlockSpec(memory_space=pl.ANY)
+    hbm = pl.BlockSpec(memory_space=pltpu.HBM)
     dma = pltpu.SemaphoreType.DMA
     block = pltpu.VMEM((planes, capacity, width), jnp.bfloat16)
     wide = pltpu.VMEM((planes, stripes, slots, width), jnp.bfloat16)
     return pl.pallas_call(
         functools.partial(mixture_kernel, capacity, stripes, slots),
-        in_specs=[vmem] * 8 + [anywhere] * 4,
+        in_specs=[vmem] * 6 + [hbm] * 6,
         out_specs=vmem,
         out_shape=jax.ShapeDtypeStruct((tok, width), jnp.bfloat16),
         scratch_shapes=[
+            pltpu.VMEM(stream.shape, stream.dtype),
+            pltpu.VMEM(route_weights.shape, route_weights.dtype),
             pltpu.VMEM(out_weight.shape, jnp.bfloat16),
             pltpu.VMEM(expert_gate.shape[1:], jnp.bfloat16),
             pltpu.VMEM(expert_up.shape[1:], jnp.bfloat16),
@@ -796,7 +864,7 @@
             wide,
             block,
             pltpu.VMEM((tok, width), jnp.float32),
-            dma((4,)),
+            dma((6,)),
             dma((planes * stripes,)),
             dma((planes * stripes,)),
             dma((planes,)),
@@ -846,7 +914,8 @@
     hits = (flat[:, None] == jnp.arange(sp_count, dtype=jnp.int32)[None, :]).astype(jnp.int32)
     slot_index = jnp.sum(jnp.cumsum(hits, axis=0) * hits, axis=1) - 1
     own_counts = jnp.sum(hits, axis=0).reshape(KV_HEADS, stripes)
-    own_offsets = jnp.cumsum(own_counts, axis=1) - own_counts
+    below = jnp.arange(stripes)[None, :, None] < jnp.arange(stripes)[None, None, :]
+    own_offsets = jnp.sum(jnp.where(below, own_counts[:, :, None], 0), axis=1)
     position = (slot_index + jnp.sum(hits * own_offsets.reshape(1, -1), axis=1)).reshape(TOP, tok)
     owner = (flat // stripes).reshape(TOP, tok)
     full = stripes * slots
@@ -869,7 +938,7 @@
     spot = lax.rem(lax.axis_index("sp"), stripes)
     counts = lax.dynamic_index_in_dim(notes_all, spot, 0, keepdims=False)
     counts = counts[:, group + 1, :stripes].astype(jnp.int32)
-    offsets = jnp.cumsum(counts, axis=1) - counts
+    offsets = jnp.sum(jnp.where(below, counts[:, :, None], 0), axis=1)
     number = jnp.arange(slots, dtype=jnp.int32)[None, None, :]
     begin = jnp.where(number < counts[:, :, None], offsets[:, :, None] + number, -1)
     begin = begin.reshape(KV_HEADS, full)
@@ -887,16 +956,16 @@
         compiler_params=pltpu.CompilerParams(vmem_limit_bytes=48 * 1024 * 1024),
         name="attend",
     )(query_got, kv_all, notes_all)
-    sizes = (full * 5 // 8, full * 11 // 16, full * 13 // 16, full)
+    sizes = tuple(full * part // 32 for part in (20, 22, 24, 32))
     operands = (
         mixed,
-        stream,
         norm_gain[None, :],
         place,
         jnp.transpose(place),
-        route_weights,
         begin[:, None, :],
         begin[:, :, None],
+        stream,
+        route_weights,
         out_weight,
         expert_gate,
         expert_up,

time: 260 us -> 234 us (0.900); the launches traced: 261 us -> 230 us
  Pallas kernels: 243 us -> 213 us
    pallas_call x1, Pallas kernels: 185 us -> 156 us  [mixture(): pl.pallas_call(functools.partial(mixture_kernel, capacity, stripes, slots...]
where the time goes in v1:
time: 234 us; the launch traced here: 230 us
  Pallas kernels  213 us (91%)
  local copies, waits for them, and re-layouts  9.65 us (4%)
  other arithmetic  5.16 us (2%)
    pallas_call x1, Pallas kernels, mixture(): pl.pallas_call(functools.partial(mixture_kernel, capacity, stripes, slots...  156 us
    pallas_call x1, Pallas kernels, fast_shards(): pl.pallas_call(functools.partial(attend_kernel, sub, span, width), grid=(...  30.7 us
    pallas_call x1, Pallas kernels, exchange(): pl.pallas_call(functools.partial(exchange_kernel, stripes), in_specs=[hbm...  27.1 us
    unnamed x14, local copies, waits for them, and re-layouts  5.84 us

profile of v1, /device:TPU:19, one launch (start us, length us, event | category | flops | bytes accessed | tf_op | source)
XLA Modules:
  0.0 230.1 jit_solution(2895728878608744430)
XLA Ops:
  0.0 0.8 reshape.205
  0.8 0.7 convert_element_type.46
  1.5 0.7 copy.115
  2.1 0.1 convert_reduce_fusion
  2.3 0.1 broadcast_in_dim_reshape.2
  2.4 0.1 reshape.206
  2.4 0.1 reduce_sum.55
  2.6 0.6 reduce_max.18
  3.9 1.0 copy-done
  5.0 0.9 copy-done.1
  5.9 0.9 copy-done.2
  6.8 27.1 %exchange.1 = (bf16[8,4,256,128]{3,2,1,0:T(8,128)(2,1)S(1)}, bf16[32,32,256]{2,1,0:T(8,128)(2,1)S(1)}, f32[8,4,8,256]{3,2,1,0:T(8,128)S(1)}) custom-call(bf16[256,256]{1,0:T(8,128)(2,1)S(1)} %copy-done.1, bf16[256,256]{1,0:T(8,128)(2,1)S(1)} %copy-done.2, bf16[256,1024]{1,0:T(8,128)(2,1)S(1)} %copy-done, f32[4,8,256]{2,1,0:T(8,128)S(1)} %concatenate.7.notes_ref), custom_call_target="tpu_custom_call" | custom-call | tf_op jit(solution)/shard_map/exchange/pallas_call | solution.py:453
  33.9 0.6 slice_reduce_fusion.1
  35.2 30.7 %attend.1 = bf16[32,32,256]{2,1,0:T(8,128)(2,1)} custom-call(bf16[32,32,256]{2,1,0:T(8,128)(2,1)S(1)} %get-tuple-element.158.query_ref, bf16[8,4,256,128]{3,2,1,0:T(8,128)(2,1)S(1)} %get-tuple-element.159.kv_ref, f32[8,4,8,256]{3,2,1,0:T(8,128)S(1)} %get-tuple-element.157.notes_ref), custom_call_target="tpu_custom_call" | custom-call | tf_op jit(solution)/shard_map/attend/pallas_call | solution.py:945
  65.9 0.1 select_reduce_fusion.1
  66.0 0.1 mul.22
  66.1 1.2 reduce-window.6
  67.3 0.2 slice_reduce_fusion
  67.5 0.1 fusion.1
  67.7 0.1 copy.109
  67.8 0.1 lt.87
  67.9 0.1 lt.93
  68.1 159.7 %conditional.1 = (bf16[256,2048]{1,0:T(8,128)(2,1)}) conditional(s32[]{:T(128)} %clamp.3, (bf16[32,32,256]{2,1,0:T(8,128)(2,1)}, f32[2048]{0:T(1024)S(1)}, s32[2,256]{1,0:T(2,128)S(1)}, s32[256,2]{1,0:T(8,128)S(1)}, s32[4,1,256]{2,1,0:T(1,128)S(1)}, /*index=5*/s32[4,256,1]{2,1,0:T(8,128)S(1)}, ...), branch_computations={%region_10.11_spmd.clone, %region_11.12_spmd.clone, %region_12.13_... | conditional | flops 6144 | bytes 73872 | solution.py:979
  68.1 0.1 lt.114
  68.3 0.1 add.91
  68.3 0.6 compare_select_fusion.begin_row_ref
  68.9 0.5 add.109
  69.5 0.5 lt.128
  70.0 0.9 add_select_fusion.begin_ref
  70.9 0.8 copy.110.weights_hbm
  71.7 155.7 %mixture.4 = bf16[256,2048]{1,0:T(8,128)(2,1)} custom-call(bf16[32,32,256]{2,1,0:T(8,128)(2,1)} %get-tuple-element.305.mixed_ref, f32[1,2048]{1,0:T(1,128)S(1)} %bitcast.33, s32[2,256]{1,0:T(2,128)S(1)} %get-tuple-element.306.rows_ref, s32[256,2]{1,0:T(8,128)S(1)} %get-tuple-element.307.columns_ref, s32[4,1,256]{2,1,0:T(1,128)} %compare_select_fusion.begin_row_ref, ...), custom_call_target="tpu_custom_call" | custom-call | tf_op jit(solution)/shard_map/cond/branch_0_fun/mixture/pallas_call | solution.py:843
  227.8 2.3 %copy.122 = bf16[256,2048]{1,0:T(8,128)(2,1)} copy(bf16[256,2048]{1,0:T(8,128)(2,1)} %get-tuple-element.160) | data formatting | bytes 2097152
  (28 shorter events, 0.4 us)
Async XLA Ops:
  0.0 66.1 %copy-start.5 = (s32[256,2]{0,1:T(2,128)S(1)}, s32[256,2]{0,1:T(2,128)}, u32[]{:S(2)}) copy-start(s32[256,2]{0,1:T(2,128)} %param.25) | copy-start | bytes 6148
  0.0 68.1 %copy-start.3 = (f32[2048]{0:T(1024)S(1)}, f32[2048]{0:T(1024)}, u32[]{:S(2)}) copy-start(f32[2048]{0:T(1024)} %param.24) | copy-start | bytes 24580
  0.0 68.1 %copy-start.4 = (f32[256,2]{0,1:T(2,128)S(1)}, f32[256,2]{0,1:T(2,128)}, u32[]{:S(2)}) copy-start(f32[256,2]{0,1:T(2,128)} %param.26) | copy-start | bytes 6148
  3.9 1.0 copy-start
  5.0 0.9 copy-start.1
  5.9 0.9 copy-start.2

commit v2 on v1

--- a/solution.py
+++ b/solution.py
@@ -290,12 +290,18 @@
     keys_hbm,
     values_hbm,
     query_ref,
-    notes_ref,
+    gates_hbm,
+    documents_hbm,
+    routes_hbm,
     kv_all_ref,
     got_ref,
     notes_all_ref,
     keys_ref,
     values_ref,
+    gates_ref,
+    documents_ref,
+    routes_ref,
+    notes_ref,
     kv_ref,
     l_sem,
     z_send,
@@ -331,12 +337,39 @@
     loads = [
         pltpu.make_async_copy(keys_hbm, keys_ref, l_sem.at[0]),
         pltpu.make_async_copy(values_hbm, values_ref, l_sem.at[1]),
+        pltpu.make_async_copy(gates_hbm, gates_ref, l_sem.at[3]),
+        pltpu.make_async_copy(documents_hbm, documents_ref, l_sem.at[4]),
+        pltpu.make_async_copy(routes_hbm, routes_ref, l_sem.at[5]),
         pltpu.make_async_copy(query_ref.at[piece(me)], got_ref.at[me], l_sem.at[2]),
     ]
     for load in loads:
         load.start()
-    for load in loads[:2]:
+    for load in loads[:5]:
         load.wait()
+    tok, part = keys_ref.shape[0], min(128, keys_ref.shape[0])
+    group = gates_ref.shape[0] // planes
+    line = lax.broadcasted_iota(jnp.int32, (part, 1), 0)
+    ones = jnp.full((8, tok), 1.0, jnp.bfloat16)
+    counts = []
+    for g in range(planes):
+        own = jnp.where(line < stripes, line + g * stripes, -1)
+        hits = sum(jnp.where(own == routes_ref[k:k + 1], 1.0, 0.0) for k in range(TOP))
+        count = lax.dot_general(
+            ones,
+            hits.astype(jnp.bfloat16),
+            (((1,), (1,)), ((), ())),
+            preferred_element_type=jnp.float32,
+        )
+        counts.append(count[:1])
+    largest = functools.reduce(
+        jnp.maximum, [jnp.sum(count, axis=1, keepdims=True) for count in counts]
+    )
+    for g in range(planes):
+        notes_ref[g] = jnp.zeros(notes_ref.shape[1:], jnp.float32)
+        notes_ref[g, 0:group] = gates_ref[g * group:(g + 1) * group]
+        notes_ref[g, group:group + 1] = documents_ref[...].astype(jnp.float32)
+        notes_ref[g, group + 1:group + 2, 0:part] = counts[g]
+        notes_ref[g, group + 2:group + 3] = jnp.broadcast_to(largest, (1, tok))
     for g in range(planes):
         part = slice(g * HD, (g + 1) * HD)
         kv_ref[g] = jnp.concatenate([keys_ref[:, part], values_ref[:, part]], axis=1)
@@ -410,7 +443,7 @@
     lax.fori_loop(1, total, send_query, 0)
     kv_all_ref[spot, plane] = kv_ref[plane]
     notes_all_ref[spot, plane] = notes_ref[plane]
-    loads[2].wait()
+    loads[5].wait()
     for at, r in enumerate(order):
         for n in both:
             along(r, n).wait_recv()
@@ -443,8 +476,13 @@
     lax.fori_loop(1, total, end_query, 0)
 
 
-def exchange(keys, values, queries, notes, stripes):
-    planes, chips = notes.shape[0], stripes // 2
+def exchange(operands, stripes):
+    keys, values, queries, gates, documents, routes = [
+        pltpu.with_memory_space_constraint(array, pltpu.HBM) for array in operands
+    ]
+    planes, chips = KV_HEADS, stripes // 2
+    rows = -(-(QUERY_HEAD_COUNT // KV_HEADS + 3) // 8) * 8
+    notes = jax.ShapeDtypeStruct((planes, rows, keys.shape[0]), jnp.float32)
     total, tok = planes * stripes, keys.shape[0]
     got = (total, tok // stripes, queries.shape[1] // planes)
     hbm = pl.BlockSpec(memory_space=pltpu.HBM)
@@ -452,7 +490,7 @@
     dma = pltpu.SemaphoreType.DMA
     return pl.pallas_call(
         functools.partial(exchange_kernel, stripes),
-        in_specs=[hbm, hbm, hbm, vmem],
+        in_specs=[hbm] * 6,
         out_specs=[vmem] * 3,
         out_shape=[
             jax.ShapeDtypeStruct((stripes, planes, tok, 2 * HD), keys.dtype),
@@ -462,8 +500,12 @@
         scratch_shapes=[
             pltpu.VMEM(keys.shape, keys.dtype),
             pltpu.VMEM(values.shape, values.dtype),
+            pltpu.VMEM(gates.shape, gates.dtype),
+            pltpu.VMEM(documents.shape, documents.dtype),
+            pltpu.VMEM(routes.shape, routes.dtype),
+            pltpu.VMEM(notes.shape, notes.dtype),
             pltpu.VMEM((planes, tok, 2 * HD), keys.dtype),
-            dma((3,)),
+            dma((6,)),
             dma((2, planes)),
             dma((2, planes)),
             dma((2, planes, chips)),
@@ -477,7 +519,7 @@
             collective_id=0, has_side_effects=True, vmem_limit_bytes=24 * 1024 * 1024
         ),
         name="exchange",
-    )(keys, values, queries, notes)
+    )(keys, values, queries, gates, documents, routes)
 
 
 def mixture_kernel(
@@ -486,19 +528,18 @@
     slots,
     mixed_ref,
     gain_ref,
-    rows_ref,
-    columns_ref,
-    begin_row_ref,
-    begin_ref,
+    routes_ref,
+    weights_ref,
+    notes_ref,
     stream_hbm,
-    weights_hbm,
     project_hbm,
     gate_hbm,
     up_hbm,
     down_hbm,
     out_ref,
     stream_ref,
-    weights_ref,
+    begin_ref,
+    rows_ref,
     project_w,
     gate_w,
     up_w,
@@ -527,7 +568,7 @@
     r_send,
     r_recv,
 ):
-    planes = begin_ref.shape[0]
+    planes = notes_ref.shape[1]
     devices = planes * stripes
     tok, width = stream_ref.shape
     sub, wide = mixed_ref.shape[1:]
@@ -556,7 +597,6 @@
         for at, (source, target) in enumerate(
             (
                 (stream_hbm, stream_ref),
-                (weights_hbm, weights_ref),
                 (project_hbm, project_w),
                 (gate_hbm.at[0], gate_w),
                 (up_hbm.at[0], up_w),
@@ -566,6 +606,41 @@
     ]
     for copy in weights:
         copy.start()
+
+    def as_bf16(hit):
+        return jnp.where(hit, 1.0, 0.0).astype(jnp.bfloat16)
+
+    def iota(shape, axis):
+        return lax.broadcasted_iota(jnp.int32, shape, axis)
+
+    def exact(left, right):
+        return jnp.dot(left, right, preferred_element_type=jnp.float32)
+
+    part = min(128, tok)
+    lane = iota((1, rows), 1)
+    number = lax.rem(lane, slots)
+    line = iota((part, rows), 0)
+    same, under = as_bf16(line == lax.div(lane, slots)), as_bf16(line < lax.div(lane, slots))
+    row = QUERY_HEAD_COUNT // KV_HEADS + 1
+    for p in range(planes):
+        told = notes_ref[spot, p][:, :part].astype(jnp.bfloat16)
+        count = exact(told, same)[row:row + 1].astype(jnp.int32)
+        start = exact(told, under)[row:row + 1].astype(jnp.int32)
+        begin_ref[p] = jnp.where(number < count, start + number, -1)
+    expert = iota((devices, 1), 0)
+    earlier = as_bf16(iota((tok, tok), 0) < iota((tok, tok), 1))
+    hits = [expert == routes_ref[k:k + 1] for k in range(TOP)]
+    before = [exact(as_bf16(hit), earlier) for hit in hits]
+    sums = [jnp.sum(jnp.where(hit, 1.0, 0.0), axis=1, keepdims=True) for hit in hits]
+    high_id, low_id = iota((devices, devices), 0), iota((devices, devices), 1)
+    inside = (lax.div(high_id, stripes) == lax.div(low_id, stripes)) & (low_id < high_id)
+    counts = jnp.broadcast_to(sum(sums), (devices, 128)).astype(jnp.bfloat16)
+    base = exact(as_bf16(inside), counts)[:, :1]
+    base = base + (lax.div(expert, stripes) * rows).astype(jnp.float32)
+    for k in range(TOP):
+        spots = jnp.where(hits[k], before[k] + base, 0.0)
+        rows_ref[k:k + 1] = jnp.sum(spots, axis=0, keepdims=True).astype(jnp.int32)
+        base = base + sums[k]
     pl.semaphore_wait(barrier, devices - 1)
 
     def home(owner):
@@ -596,7 +671,7 @@
     lax.fori_loop(1, devices, send_home, 0)
     attended[home(me)] = mixed_ref[me]
     lax.fori_loop(1, devices, wait_home, 0)
-    for copy in weights[:3]:
+    for copy in weights[:2]:
         copy.wait()
 
     def project(index, squares):
@@ -627,10 +702,14 @@
 
     columns(norm, width, step)
     high_slot = lax.broadcasted_iota(jnp.int32, (capacity, 1), 0)
-    low_slot = lax.broadcasted_iota(jnp.int32, (1, capacity), 1)
 
     def chosen_of(hit):
         return jnp.where(hit, 1.0, 0.0)
+
+    def turned_dot(left, right):
+        return lax.dot_general(
+            left, right, (((0,), (0,)), ((), ())), preferred_element_type=jnp.float32
+        )
 
     def out_copy(m):
         return pltpu.make_async_remote_copy(
@@ -684,14 +763,14 @@
         lax.fori_loop(1, stripes, at, 0)
 
     def spread(m):
-        hits = chosen_of(begin_ref[plane_of(m)] == low_slot).astype(jnp.bfloat16)
+        hits = chosen_of(begin_ref[plane_of(m)] == high_slot).astype(jnp.bfloat16)
 
         @pl.when(m > 0)
         def wait():
             out_copy(m).wait_recv()
 
         def body(cols):
-            chosen = dot(hits, landed[m, :, cols]).astype(jnp.bfloat16)
+            chosen = turned_dot(hits, landed[m, :, cols]).astype(jnp.bfloat16)
             sending[m, :, :, cols] = chosen.reshape(stripes, slots, step)
 
         columns(body, width, step)
@@ -719,7 +798,7 @@
         peers(lambda i: from_expert(m, i).start())
 
     def collect(m):
-        hits = chosen_of(begin_row_ref[plane_of(m)] == high_slot).astype(jnp.bfloat16)
+        hits = chosen_of(begin_ref[plane_of(m)] == high_slot).astype(jnp.bfloat16)
         peers(lambda i: from_expert(m, i).wait_recv())
 
         def body(cols):
@@ -735,7 +814,7 @@
     def combine(m, final):
         begins = plane_of(m) * rows
         share = sum(
-            jnp.where(columns_ref[:, k:k + 1] - begins == low_slot, weights_ref[:, k:k + 1], 0.0)
+            jnp.where(rows_ref[k:k + 1] - begins == high_slot, weights_ref[k:k + 1], 0.0)
             for k in range(TOP)
         )
         high = share.astype(jnp.bfloat16)
@@ -743,7 +822,7 @@
 
         def body(cols):
             rows_got = got[m, :, cols]
-            term = total[:, cols] + dot(high, rows_got) + dot(low, rows_got)
+            term = total[:, cols] + turned_dot(high, rows_got) + turned_dot(low, rows_got)
             if final:
                 out_ref[:, cols] = term.astype(jnp.bfloat16)
             else:
@@ -787,7 +866,7 @@
 
         @pl.when(q == 0)
         def ready():
-            for copy in weights[3:]:
+            for copy in weights[2:]:
                 copy.wait()
 
         @pl.when(q == 3)
@@ -831,10 +910,9 @@
 
 
 def mixture(capacity, stripes, slots, operands):
-    begin = operands[5]
-    stream, route_weights, out_weight, expert_gate, expert_up, expert_down = operands[6:]
+    stream, out_weight, expert_gate, expert_up, expert_down = operands[5:]
     tok, width = stream.shape
-    planes = begin.shape[0]
+    planes = operands[4].shape[1]
     vmem = pl.BlockSpec(memory_space=pltpu.VMEM)
     hbm = pl.BlockSpec(memory_space=pltpu.HBM)
     dma = pltpu.SemaphoreType.DMA
@@ -842,12 +920,13 @@
     wide = pltpu.VMEM((planes, stripes, slots, width), jnp.bfloat16)
     return pl.pallas_call(
         functools.partial(mixture_kernel, capacity, stripes, slots),
-        in_specs=[vmem] * 6 + [hbm] * 6,
+        in_specs=[vmem] * 5 + [hbm] * 5,
         out_specs=vmem,
         out_shape=jax.ShapeDtypeStruct((tok, width), jnp.bfloat16),
         scratch_shapes=[
             pltpu.VMEM(stream.shape, stream.dtype),
-            pltpu.VMEM(route_weights.shape, route_weights.dtype),
+            pltpu.VMEM((planes, 1, stripes * slots), jnp.int32),
+            pltpu.VMEM((TOP, tok), jnp.int32),
             pltpu.VMEM(out_weight.shape, jnp.bfloat16),
             pltpu.VMEM(expert_gate.shape[1:], jnp.bfloat16),
             pltpu.VMEM(expert_up.shape[1:], jnp.bfloat16),
@@ -864,7 +943,7 @@
             wide,
             block,
             pltpu.VMEM((tok, width), jnp.float32),
-            dma((6,)),
+            dma((5,)),
             dma((planes * stripes,)),
             dma((planes * stripes,)),
             dma((planes,)),
@@ -877,7 +956,7 @@
             dma((planes,)),
         ],
         compiler_params=pltpu.CompilerParams(
-            collective_id=1 + capacity // 16,
+            collective_id=1 + capacity // 8,
             has_side_effects=True,
             vmem_limit_bytes=63 * 1024 * 1024,
         ),
@@ -910,38 +989,19 @@
     width = min(span, 1024)
     tiles = sp_count // blocks
     slots = max(2, 2 * tok * TOP // sp_count)
-    flat = jnp.transpose(routes).reshape(-1)
-    hits = (flat[:, None] == jnp.arange(sp_count, dtype=jnp.int32)[None, :]).astype(jnp.int32)
-    slot_index = jnp.sum(jnp.cumsum(hits, axis=0) * hits, axis=1) - 1
-    own_counts = jnp.sum(hits, axis=0).reshape(KV_HEADS, stripes)
-    below = jnp.arange(stripes)[None, :, None] < jnp.arange(stripes)[None, None, :]
-    own_offsets = jnp.sum(jnp.where(below, own_counts[:, :, None], 0), axis=1)
-    position = (slot_index + jnp.sum(hits * own_offsets.reshape(1, -1), axis=1)).reshape(TOP, tok)
-    owner = (flat // stripes).reshape(TOP, tok)
     full = stripes * slots
-    place = owner * full + position
-    largest = jnp.max(jnp.sum(own_counts, axis=1))
-    pad = jnp.zeros((KV_HEADS, 1, tok - stripes), jnp.int32)
-    told = [
-        jnp.broadcast_to(documents[None, None, :], (KV_HEADS, 1, tok)),
-        jnp.concatenate([own_counts[:, None, :], pad], axis=2),
-        jnp.broadcast_to(largest, (KV_HEADS, 1, tok)),
-        jnp.zeros((KV_HEADS, 1, tok), jnp.int32),
-    ]
-    notes = jnp.concatenate(
-        [jnp.transpose(gate_totals).reshape(KV_HEADS, group, tok)]
-        + [line.astype(jnp.float32) for line in told],
-        axis=1,
-    )
-    kv_all, query_got, notes_all = exchange(keys, values, queries, notes, stripes)
+    kv_all, query_got, notes_all = exchange(
+        (
+            keys,
+            values,
+            queries,
+            jnp.transpose(gate_totals),
+            documents[None, :],
+            jnp.transpose(routes),
+        ),
+        stripes,
+    )
     worst = jnp.max(notes_all[:, :, group + 2, 0]).astype(jnp.int32)
-    spot = lax.rem(lax.axis_index("sp"), stripes)
-    counts = lax.dynamic_index_in_dim(notes_all, spot, 0, keepdims=False)
-    counts = counts[:, group + 1, :stripes].astype(jnp.int32)
-    offsets = jnp.sum(jnp.where(below, counts[:, :, None], 0), axis=1)
-    number = jnp.arange(slots, dtype=jnp.int32)[None, None, :]
-    begin = jnp.where(number < counts[:, :, None], offsets[:, :, None] + number, -1)
-    begin = begin.reshape(KV_HEADS, full)
     mixed = pl.pallas_call(
         functools.partial(attend_kernel, sub, span, width),
         grid=(tiles,),
@@ -956,16 +1016,14 @@
         compiler_params=pltpu.CompilerParams(vmem_limit_bytes=48 * 1024 * 1024),
         name="attend",
     )(query_got, kv_all, notes_all)
-    sizes = tuple(full * part // 32 for part in (20, 22, 24, 32))
+    sizes = tuple(full * part // 32 for part in (19, 20, 21, 22, 24, 32))
     operands = (
         mixed,
         norm_gain[None, :],
-        place,
-        jnp.transpose(place),
-        begin[:, None, :],
-        begin[:, :, None],
+        jnp.transpose(routes),
+        jnp.transpose(route_weights),
+        notes_all,
         stream,
-        route_weights,
         out_weight,
         expert_gate,
         expert_up,

time: 234 us -> 221 us (0.944)
  the two profiles are of different devices: /device:TPU:19 before, /device:TPU:0 now
where the time goes in v2:
time: 221 us; the launch traced here: 219 us
  Pallas kernels  215 us (97%)
  local copies, waits for them, and re-layouts  2.32 us (1%)
    pallas_call x1, Pallas kernels, mixture(): pl.pallas_call(functools.partial(mixture_kernel, capacity, stripes, slots...  157 us
    pallas_call x1, Pallas kernels, exchange(): pl.pallas_call(functools.partial(exchange_kernel, stripes), in_specs=[hbm...  30.1 us
    pallas_call x1, Pallas kernels, fast_shards(): pl.pallas_call(functools.partial(attend_kernel, sub, span, width), grid=(...  28.3 us

profile of v2, /device:TPU:0, one launch (start us, length us, event | category | flops | bytes accessed | tf_op | source)
XLA Modules:
  0.0 219.5 jit_solution(1643596894523285860)
XLA Ops:
  0.0 0.0 copy-start.2
  0.0 0.0 copy-start.1
  0.0 0.0 copy-start
  0.0 30.1 %exchange.1 = (bf16[8,4,256,128]{3,2,1,0:T(8,128)(2,1)S(1)}, bf16[32,32,256]{2,1,0:T(8,128)(2,1)S(1)}, f32[8,4,8,256]{3,2,1,0:T(8,128)S(1)}) custom-call(bf16[256,256]{1,0:T(8,128)(2,1)} %keys_hbm.1, bf16[256,256]{1,0:T(8,128)(2,1)} %values_hbm.1, bf16[256,1024]{1,0:T(8,128)(2,1)} %query_ref.1, f32[16,256]{1,0:T(8,128)} %bitcast.29, s32[1,256]{1,0:T(1,128)} %bitcast.30, ...), custom_call_target="tpu_custom_call" | custom-call | tf_op jit(solution)/shard_map/exchange/pallas_call | solution.py:491
  30.1 0.6 slice_reduce_fusion
  31.4 28.3 %attend.1 = bf16[32,32,256]{2,1,0:T(8,128)(2,1)S(1)} custom-call(bf16[32,32,256]{2,1,0:T(8,128)(2,1)S(1)} %get-tuple-element.196.query_ref, bf16[8,4,256,128]{3,2,1,0:T(8,128)(2,1)S(1)} %get-tuple-element.197.kv_ref, f32[8,4,8,256]{3,2,1,0:T(8,128)S(1)} %get-tuple-element.195.notes_ref), custom_call_target="tpu_custom_call" | custom-call | tf_op jit(solution)/shard_map/attend/pallas_call | solution.py:1005
  59.7 0.0 copy-done.2
  59.7 0.0 copy-done.1
  59.7 0.0 copy-done
  59.7 157.5 %conditional.1 = (bf16[256,2048]{1,0:T(8,128)(2,1)}) conditional(s32[]{:T(128)} %clamp.3, (bf16[32,32,256]{2,1,0:T(8,128)(2,1)S(1)}, f32[2048]{0:T(1024)S(1)}, s32[2,256]{1,0:T(2,128)S(1)}, f32[2,256]{1,0:T(2,128)S(1)}, f32[8,4,8,256]{3,2,1,0:T(8,128)S(1)}, /*index=5*/bf16[256,2048]{1,0:T(8,128)(2,1)}, ...), branch_computations={%region_1.0_spmd, %region_2.0_spmd, %region_3.0_spmd, %region_4.0_... | conditional | bytes 8 | solution.py:1037
  59.9 156.7 %mixture.8 = bf16[256,2048]{1,0:T(8,128)(2,1)} custom-call(bf16[32,32,256]{2,1,0:T(8,128)(2,1)S(1)} %get-tuple-element.152.mixed_ref, f32[1,2048]{1,0:T(1,128)S(1)} %bitcast.12, s32[2,256]{1,0:T(2,128)S(1)} %get-tuple-element.154.routes_ref, f32[2,256]{1,0:T(2,128)S(1)} %get-tuple-element.155.weights_ref, f32[8,4,8,256]{3,2,1,0:T(8,128)S(1)} %get-tuple-element.156.notes_ref, ...), custom_call_target="tpu_custom_call" | custom-call | tf_op jit(solution)/shard_map/cond/branch_2_fun/mixture/pallas_call | solution.py:921
  217.2 2.3 %copy.63 = bf16[256,2048]{1,0:T(8,128)(2,1)} copy(bf16[256,2048]{1,0:T(8,128)(2,1)} %get-tuple-element.198) | data formatting | bytes 2097152
Async XLA Ops:
  0.0 59.7 %copy-start.2 = (f32[256,2]{0,1:T(2,128)S(1)}, f32[256,2]{0,1:T(2,128)}, u32[]{:S(2)}) copy-start(f32[256,2]{0,1:T(2,128)} %param.28) | copy-start | bytes 6148
  0.0 59.7 %copy-start.1 = (s32[256,2]{0,1:T(2,128)S(1)}, s32[256,2]{0,1:T(2,128)}, u32[]{:S(2)}) copy-start(s32[256,2]{0,1:T(2,128)} %param.27) | copy-start | bytes 6148
  0.0 59.7 %copy-start = (f32[2048]{0:T(1024)S(1)}, f32[2048]{0:T(1024)}, u32[]{:S(2)}) copy-start(f32[2048]{0:T(1024)} %param.26) | copy-start | bytes 24580

commit v3 on v2

--- a/solution.py
+++ b/solution.py
@@ -15,7 +15,7 @@
 
 
 EPS = 1e-06
-STEP = 1024
+STEP = 2048
 MASKED = -1e30
 
 
@@ -787,7 +787,7 @@
             upper = dot(rows_in, up_w[:, cols])
             inner[:, cols] = (jax.nn.silu(gate) * upper).astype(jnp.bfloat16)
 
-        columns(middle, hidden_units, math.gcd(hidden_units, 256))
+        columns(middle, hidden_units, math.gcd(hidden_units, 512))
 
         def last(cols):
             answer = dot(inner[...], down_w[:, cols]).astype(jnp.bfloat16)
@@ -1016,7 +1016,7 @@
         compiler_params=pltpu.CompilerParams(vmem_limit_bytes=48 * 1024 * 1024),
         name="attend",
     )(query_got, kv_all, notes_all)
-    sizes = tuple(full * part // 32 for part in (19, 20, 21, 22, 24, 32))
+    sizes = tuple(full * part // 32 for part in (20, 22, 24, 32))
     operands = (
         mixed,
         norm_gain[None, :],

time: 221 us -> 228 us (1.032)
  the two profiles are of different devices: /device:TPU:0 before, /device:TPU:19 now
where the time goes in v3:
time: 228 us; the launch traced here: 227 us
  Pallas kernels  222 us (97%)
  local copies, waits for them, and re-layouts  2.32 us (1%)
    pallas_call x1, Pallas kernels, mixture(): pl.pallas_call(functools.partial(mixture_kernel, capacity, stripes, slots...  165 us
    pallas_call x1, Pallas kernels, fast_shards(): pl.pallas_call(functools.partial(attend_kernel, sub, span, width), grid=(...  30 us
    pallas_call x1, Pallas kernels, exchange(): pl.pallas_call(functools.partial(exchange_kernel, stripes), in_specs=[hbm...  27.3 us

profile of v3, /device:TPU:19, one launch (start us, length us, event | category | flops | bytes accessed | tf_op | source)
XLA Modules:
  0.0 226.8 jit_solution(13042535594372721306)
XLA Ops:
  0.0 0.0 copy-start.2
  0.0 0.0 copy-start.1
  0.0 0.0 copy-start
  0.0 27.3 %exchange.1 = (bf16[8,4,256,128]{3,2,1,0:T(8,128)(2,1)S(1)}, bf16[32,32,256]{2,1,0:T(8,128)(2,1)S(1)}, f32[8,4,8,256]{3,2,1,0:T(8,128)S(1)}) custom-call(bf16[256,256]{1,0:T(8,128)(2,1)} %keys_hbm.1, bf16[256,256]{1,0:T(8,128)(2,1)} %values_hbm.1, bf16[256,1024]{1,0:T(8,128)(2,1)} %query_ref.1, f32[16,256]{1,0:T(8,128)} %bitcast.21, s32[1,256]{1,0:T(1,128)} %bitcast.22, ...), custom_call_target="tpu_custom_call" | custom-call | tf_op jit(solution)/shard_map/exchange/pallas_call | solution.py:491
  27.3 0.6 slice_reduce_fusion
  28.6 30.0 %attend.1 = bf16[32,32,256]{2,1,0:T(8,128)(2,1)S(1)} custom-call(bf16[32,32,256]{2,1,0:T(8,128)(2,1)S(1)} %get-tuple-element.134.query_ref, bf16[8,4,256,128]{3,2,1,0:T(8,128)(2,1)S(1)} %get-tuple-element.135.kv_ref, f32[8,4,8,256]{3,2,1,0:T(8,128)S(1)} %get-tuple-element.133.notes_ref), custom_call_target="tpu_custom_call" | custom-call | tf_op jit(solution)/shard_map/attend/pallas_call | solution.py:1005
  58.6 0.0 copy-done.2
  58.6 0.0 copy-done.1
  58.6 0.0 copy-done
  58.6 165.9 %conditional.1 = (bf16[256,2048]{1,0:T(8,128)(2,1)}) conditional(s32[]{:T(128)} %clamp.3, (bf16[32,32,256]{2,1,0:T(8,128)(2,1)S(1)}, f32[2048]{0:T(1024)S(1)}, s32[2,256]{1,0:T(2,128)S(1)}, f32[2,256]{1,0:T(2,128)S(1)}, f32[8,4,8,256]{3,2,1,0:T(8,128)S(1)}, /*index=5*/bf16[256,2048]{1,0:T(8,128)(2,1)}, ...), branch_computations={%region_1.0_spmd, %region_2.0_spmd, %region_3.0_spmd, %region_4.0_... | conditional | bytes 8 | solution.py:1037
  58.8 165.1 %mixture.5 = bf16[256,2048]{1,0:T(8,128)(2,1)} custom-call(bf16[32,32,256]{2,1,0:T(8,128)(2,1)S(1)} %get-tuple-element.100.mixed_ref, f32[1,2048]{1,0:T(1,128)S(1)} %bitcast.9, s32[2,256]{1,0:T(2,128)S(1)} %get-tuple-element.102.routes_ref, f32[2,256]{1,0:T(2,128)S(1)} %get-tuple-element.103.weights_ref, f32[8,4,8,256]{3,2,1,0:T(8,128)S(1)} %get-tuple-element.104.notes_ref, ...), custom_call_target="tpu_custom_call" | custom-call | tf_op jit(solution)/shard_map/cond/branch_1_fun/mixture/pallas_call | solution.py:921
  224.5 2.3 %copy.47 = bf16[256,2048]{1,0:T(8,128)(2,1)} copy(bf16[256,2048]{1,0:T(8,128)(2,1)} %get-tuple-element.136) | data formatting | bytes 2097152
Async XLA Ops:
  0.0 58.6 %copy-start.2 = (f32[256,2]{0,1:T(2,128)S(1)}, f32[256,2]{0,1:T(2,128)}, u32[]{:S(2)}) copy-start(f32[256,2]{0,1:T(2,128)} %param.26) | copy-start | bytes 6148
  0.0 58.6 %copy-start.1 = (s32[256,2]{0,1:T(2,128)S(1)}, s32[256,2]{0,1:T(2,128)}, u32[]{:S(2)}) copy-start(s32[256,2]{0,1:T(2,128)} %param.25) | copy-start | bytes 6148
  0.0 58.6 %copy-start = (f32[2048]{0:T(1024)S(1)}, f32[2048]{0:T(1024)}, u32[]{:S(2)}) copy-start(f32[2048]{0:T(1024)} %param.24) | copy-start | bytes 24580
